TPU v7x, 32 devices: a whole 2x2x4 slice. The times are simulated.
32 devices in a mesh: grp: 2 (over y), dp: 2 (over x), kv: 4 (over z), tp: 2 (over core).
Axes of the slice: x: 2, y: 2, z: 4, core: 2. Of those that a mesh axis runs over, the one named last changes fastest.
Arguments:
- queries: bfloat16 [4, 1024, 2048], P(('grp', 'dp'), 'kv', 'tp'), parts along dimension 0, may hold values from -10 to 10
- keys: bfloat16 [4, 1024, 512], P(('grp', 'dp'), 'kv', 'tp'), parts along dimension 0, may hold values from -10 to 10
- values: bfloat16 [4, 1024, 512], P(('grp', 'dp'), 'kv', 'tp'), parts along dimension 0, may hold values from -6 to 6
- gate_logits: float32 [4, 2, 1024, 32], P(('grp', 'dp'), None, 'kv', 'tp'), parts along dimension 0, may hold values from -6 to 6
- chosen: int32 [4, 8, 8, 16], P(('grp', 'dp'), 'kv', 'tp'), parts along dimension 0, may hold values from -1 to 15, as said below
- pool_k: float32 [32, 64], replicated, may hold values from 0 to 0.35
- pool_v: float32 [32, 64], replicated, may hold values from 0 to 0.35
- out_gain: float32 [2048], P('tp'), may hold values from 0.1 to 1.9
Outputs:
- attended: bfloat16 [4, 1024, 2048], P(('grp', 'dp'), 'kv', 'tp'), parts along dimension 0
There are 2 independent parts, one for each index of `grp`. A program takes and returns all parts, laid end to end along the dimension named above; an argument that names none is the same for every part. Nothing has to cross between parts.
Inputs may be any that keep to these rules, and one draw needn't show every extreme that they name: Entries are key block numbers (block e holds positions e * 64 to e * 64 + 63) or -1 for none. The list of query block b (positions b * 128 onward) holds the blocks that contain its own positions, other distinct blocks that begin before it, and -1 in its remaining entries. For the query blocks of one span of 256 positions and one key head, the blocks chosen from any other span number at most 2; in every draw some span reaches 2.
All inputs are finite; a program needn't handle non-finite values.
Results may differ from a plain program's by a relative error of at most 0.0079.
Values may be sent and summed in bfloat16 or wider, within the bound.
A program may use at most 64 MiB of HBM per device.

v0:
```python
import jax
import jax.numpy as jnp
from jax import lax
from jax.sharding import PartitionSpec as P

DH = 64
CMP_STRIDE = 16
CMP_BLOCK = 32
SLC = 64
QB = 128
NSEL = 16
MOST = 2
THETA = 500000.0
EPS = 1e-06
NEG = -1e30


def shifted(block, axis, distance):
    devices = range(lax.axis_size(axis))
    route = [(i - distance, i) for i in devices if i - distance in devices]
    return lax.ppermute(block, axis, route)


def rotate(matrix, start, heads):
    length = matrix.shape[0]
    half = DH // 2
    place = (start + jnp.arange(length)).astype(jnp.float32)
    freq = jnp.power(jnp.float32(THETA), -(2.0 * jnp.arange(half).astype(jnp.float32)) / DH)
    angle = place[:, None] * freq[None, :]
    cosine = jnp.cos(angle)[:, None, :]
    sine = jnp.sin(angle)[:, None, :]
    parts = matrix.reshape(length, heads, DH).astype(jnp.float32)
    first = parts[..., :half]
    second = parts[..., half:]
    turned = jnp.concatenate([first * cosine - second * sine, second * cosine + first * sine], -1)
    return turned.reshape(length, heads * DH).astype(jnp.bfloat16)


def compress(extended, pool, groups):
    count = extended.shape[0] // CMP_STRIDE - 1
    parts = extended.reshape(count + 1, CMP_STRIDE, groups, DH).astype(jnp.float32)
    lower = jnp.einsum(
        "nigd,id->ngd", parts[:-1], pool[:CMP_STRIDE], precision=lax.Precision.HIGHEST
    )
    upper = jnp.einsum(
        "nigd,id->ngd", parts[1:], pool[CMP_STRIDE:], precision=lax.Precision.HIGHEST
    )
    return (lower + upper).astype(jnp.bfloat16)


def wanted_blocks(lists, owners, per_owner):
    groups = lists.shape[1]
    total = owners * per_owner
    hits = lists[..., None] == jnp.arange(total, dtype=jnp.int32)
    member = jnp.any(hits, axis=(0, 2)).astype(jnp.int32).reshape(groups, owners, per_owner)
    rank = jnp.cumsum(member, -1) - member
    slot_hit = (member[..., None] == 1) & (rank[..., None] == jnp.arange(MOST))
    local_ids = jnp.arange(per_owner, dtype=jnp.int32)[:, None]
    asked = jnp.sum(jnp.where(slot_hit, local_ids, 0), axis=2)
    return (asked.transpose(1, 0, 2), rank.reshape(groups, total))


def per_device(queries, keys, values, gate_logits, chosen, pool_k, pool_v, out_gain):
    queries = queries[0]
    keys = keys[0]
    values = values[0]
    logits = gate_logits[0]
    lists = chosen[0]
    length = queries.shape[0]
    groups = keys.shape[1] // DH
    heads = queries.shape[1] // DH
    per_group = heads // groups
    qblocks = length // QB
    owners = lax.axis_size("kv")
    myself = lax.axis_index("kv")
    start = myself * length
    scale = DH ** (-0.5)
    query_turned = rotate(queries, start, heads)
    key_turned = rotate(keys, start, groups)
    next_keys, next_values = shifted((keys[:CMP_STRIDE], values[:CMP_STRIDE]), "kv", -1)
    key_summary = compress(jnp.concatenate([keys, next_keys], 0), pool_k, groups)
    value_summary = compress(jnp.concatenate([values, next_values], 0), pool_v, groups)
    place = start + jnp.arange(length)
    query_group = queries.reshape(length, groups, per_group, DH).transpose(1, 2, 0, 3)
    part_keys = lax.all_gather(key_summary, "kv", axis=0, tiled=True)
    part_values = lax.all_gather(value_summary, "kv", axis=0, tiled=True)
    count = part_keys.shape[0]
    ends = jnp.arange(count) * CMP_STRIDE + CMP_BLOCK - 1
    allow = ends[None, :] <= place[:, None]

    def per_group_fold(item):
        query_part, key_part, value_part, top, total, summed = item
        score = (
            jnp.einsum("htd,nd->htn", query_part, key_part, preferred_element_type=jnp.float32)
            * scale
        )
        score = jnp.where(allow, score, NEG)
        fresh = jnp.maximum(top, jnp.max(score, -1))
        weight = jnp.where(allow, jnp.exp(score - fresh[..., None]), 0.0)
        shrink = jnp.exp(top - fresh)
        total = total * shrink + jnp.sum(weight, -1)
        summed = summed * shrink[..., None] + jnp.einsum(
            "htn,nd->htd",
            weight.astype(jnp.bfloat16),
            value_part,
            preferred_element_type=jnp.float32,
        )
        return (fresh, total, summed)

    top = jnp.full((groups, per_group, length), NEG, jnp.float32)
    total = jnp.zeros((groups, per_group, length), jnp.float32)
    summed = jnp.zeros((groups, per_group, length, DH), jnp.float32)
    top, total, summed = lax.map(
        per_group_fold,
        (
            query_group,
            part_keys.transpose(1, 0, 2),
            part_values.transpose(1, 0, 2),
            top,
            total,
            summed,
        ),
    )
    summary_out = summed / jnp.maximum(total, 1.0)[..., None]
    group_pick = jnp.arange(groups)[None, :, None]
    safe = jnp.maximum(lists, 0)
    per_owner = length // SLC
    asked_ids, rank = wanted_blocks(lists, owners, per_owner)
    requests = lax.all_to_all(asked_ids, "kv", split_axis=0, concat_axis=0, tiled=True)
    local_keys = key_turned.reshape(per_owner, SLC, groups, DH)
    local_values = values.reshape(per_owner, SLC, groups, DH)
    served = (local_keys[requests, :, group_pick, :], local_values[requests, :, group_pick, :])
    got_keys, got_values = (
        lax.all_to_all(served[0], "kv", split_axis=0, concat_axis=0, tiled=True),
        lax.all_to_all(served[1], "kv", split_axis=0, concat_axis=0, tiled=True),
    )

    def table(received, local):
        remote = received.transpose(1, 0, 2, 3, 4).reshape(groups, owners * MOST, SLC, DH)
        return jnp.concatenate([remote, local.transpose(2, 0, 1, 3)], 1)

    owner = safe // per_owner
    inner = safe % per_owner
    slot = jnp.where(owner == myself, owners * MOST + inner, owner * MOST + rank[group_pick, safe])
    key_sel = table(got_keys, local_keys)[group_pick, slot]
    value_sel = table(got_values, local_values)[group_pick, slot]
    query_blocks = query_turned.reshape(qblocks, QB, groups, per_group, DH)

    def attend(item):
        index, query_part, keys_part, values_part, picks = item
        place_q = start + index * QB + jnp.arange(QB)
        score = jnp.einsum(
            "tghd,gnkd->ghtnk", query_part, keys_part, preferred_element_type=jnp.float32
        )
        score = score.reshape(groups, per_group, QB, NSEL * SLC) * scale
        safe_picks = jnp.maximum(picks, 0)
        key_place = (safe_picks[..., None] * SLC + jnp.arange(SLC)).reshape(groups, NSEL * SLC)
        live = jnp.broadcast_to(picks[..., None] >= 0, (groups, NSEL, SLC)).reshape(
            groups, NSEL * SLC
        )
        allow = (live[:, None, :] & (key_place[:, None, :] <= place_q[None, :, None]))[:, None]
        score = jnp.where(allow, score, NEG)
        top_sel = jnp.max(score, -1, keepdims=True)
        weight = jnp.where(allow, jnp.exp(score - top_sel), 0.0)
        total_sel = jnp.sum(weight, -1)
        flat_values = values_part.reshape(groups, NSEL * SLC, DH)
        out = jnp.einsum(
            "ghtk,gkd->ghtd",
            weight.astype(jnp.bfloat16),
            flat_values,
            preferred_element_type=jnp.float32,
        )
        return out / total_sel[..., None]

    chosen_out = lax.map(attend, (jnp.arange(qblocks), query_blocks, key_sel, value_sel, lists))
    gates = jax.nn.sigmoid(logits)
    summary_rows = summary_out.transpose(2, 0, 1, 3).reshape(length, heads, DH)
    chosen_rows = chosen_out.transpose(0, 3, 1, 2, 4).reshape(length, heads, DH)
    mixed = gates[0][..., None] * summary_rows + gates[1][..., None] * chosen_rows
    normed = (
        mixed
        * lax.rsqrt(jnp.mean(mixed * mixed, -1, keepdims=True) + EPS)
        * out_gain.reshape(heads, DH)
    )
    return normed.reshape(1, length, heads * DH).astype(jnp.bfloat16)


def solution(mesh):
    in_specs = (
        P(("grp", "dp"), "kv", "tp"),
        P(("grp", "dp"), "kv", "tp"),
        P(("grp", "dp"), "kv", "tp"),
        P(("grp", "dp"), None, "kv", "tp"),
        P(("grp", "dp"), "kv", "tp", None),
        P(),
        P(),
        P("tp"),
    )
    out_specs = P(("grp", "dp"), "kv", "tp")
    return jax.shard_map(
        per_device, mesh=mesh, in_specs=in_specs, out_specs=out_specs, check_vma=False
    )
```

profile of v0, /device:TPU:0, one launch (start us, length us, event | category | flops | bytes accessed | tf_op | source)
XLA Modules:
  0.0 114.5 jit_solution(15482757723917872336)
XLA Ops:
  0.0 0.8 fusion.37
  0.9 0.7 reduce_window_sum.13
  1.7 0.2 select_reduce_fusion.2
  1.9 0.7 copy.74
  2.6 6.3 %all-to-all-start = ((s32[4,4,2]{1,2,0:T(2,128)}), s32[4,4,2]{1,2,0:T(2,128)S(1)}, u32[]{:S(2)}, u32[]{:S(2)}) async-start(s32[4,4,2]{1,2,0:T(2,128)} %copy.74), calls=%async_computation | async-start | bytes 8192 | tf_op jit(solution)/shard_map/all_to_all | solution.py:129
  8.9 0.7 slice_bitcast_fusion.1
  9.6 1.3 %collective-permute-start.1 = (bf16[16,256]{1,0:T(8,128)(2,1)S(1)}, bf16[16,256]{1,0:T(8,128)(2,1)S(1)}, u32[]{:S(2)}, u32[]{:S(2)}) collective-permute-start(bf16[16,256]{1,0:T(8,128)(2,1)S(1)} %slice_bitcast_fusion.1), channel_id=1, source_target_pairs={{2,0},{4,2},{6,4},{3,1},{5,3},{7,5},{10,8},{12,10},{14,12},{11,9},... | collective-permute-start | bytes 24584 | tf_op jit(solution)/shard_map/ppermute | solution.py:21
  10.9 0.7 slice_bitcast_fusion.4
  11.6 1.3 %collective-permute-start = (bf16[16,256]{1,0:T(8,128)(2,1)S(1)}, bf16[16,256]{1,0:T(8,128)(2,1)S(1)}, u32[]{:S(2)}, u32[]{:S(2)}) collective-permute-start(bf16[16,256]{1,0:T(8,128)(2,1)S(1)} %slice_bitcast_fusion.4), channel_id=1, source_target_pairs={{2,0},{4,2},{6,4},{3,1},{5,3},{7,5},{10,8},{12,10},{14,12},{11,9},... | collective-permute-start | bytes 24584 | tf_op jit(solution)/shard_map/ppermute | solution.py:21
  13.0 0.7 bitcast_or_fusion
  13.7 1.0 copy.73
  14.8 1.1 reshape_squeeze.9
  15.8 1.1 slice.65
  16.9 1.1 slice.72
  18.1 1.5 %gather_fusion.1 = s32[128]{0:T(128)S(1)} fusion(s32[4,16]{1,0:T(4,128)S(1)} %convert_subtract_fusion, s32[128]{0:T(128)S(1)} %reshape.454), kind=kCustom, calls=%fused_computation.1 | custom fusion | bytes 2048 | tf_op jit(solution)/shard_map/gather | solution.py:144
  19.7 0.7 fusion.46
  20.5 0.7 slice_bitcast_fusion.5
  21.3 0.7 slice_bitcast_fusion
  22.0 0.8 add_divide_fusion
  23.4 0.2 copy.77
  24.5 0.2 copy.79
  24.9 0.9 copy.84
  26.0 0.7 gather_fusion.3
  26.7 1.1 reshape.513
  27.8 7.4 %all-to-all-start.2 = ((bf16[4,2,16384]{2,1,0:T(2,128)(2,1)}), bf16[4,2,16384]{2,1,0:T(2,128)(2,1)S(1)}, u32[]{:S(2)}, u32[]{:S(2)}) async-start(bf16[4,2,16384]{2,1,0:T(2,128)(2,1)} %reshape.513), calls=%async_computation.2 | async-start | bytes 524288 | tf_op jit(solution)/shard_map/all_to_all | solution.py:135
  35.3 0.7 gather_fusion
  35.9 1.1 reshape.511
  37.6 13.7 %all_gather.7 = bf16[64,4,64]{2,1,0:T(4,128)(2,1)S(1)} all-gather(bf16[16,4,64]{2,1,0:T(4,128)(2,1)S(1)} %fusion.39), channel_id=1, replica_groups=mesh['grp'=2,'dp'=2,'kv'=4,'tp'=2] {'kv'}, dimensions={0}, use_global_device_ids=true | all-gather | bytes 40960 | tf_op jit(solution)/shard_map/all_gather | solution.py:86
  51.6 13.3 %all_gather.6 = bf16[64,4,64]{2,0,1:T(8,128)(2,1)S(1)} all-gather(bf16[16,4,64]{2,0,1:T(8,128)(2,1)S(1)} %fusion.40), channel_id=1, replica_groups=mesh['grp'=2,'dp'=2,'kv'=4,'tp'=2] {'kv'}, dimensions={0}, use_global_device_ids=true | all-gather | bytes 40960 | tf_op jit(solution)/shard_map/all_gather | solution.py:85
  64.9 4.6 %all-to-all-start.1 = ((bf16[4,2,16384]{2,1,0:T(2,128)(2,1)}), bf16[4,2,16384]{2,1,0:T(2,128)(2,1)S(1)}, u32[]{:S(2)}, u32[]{:S(2)}) async-start(bf16[4,2,16384]{2,1,0:T(2,128)(2,1)} %reshape.511), calls=%async_computation.1 | async-start | bytes 524288 | tf_op jit(solution)/shard_map/all_to_all | solution.py:134
  69.5 5.2 %while.24 = (s32[]{:T(128)}, f32[4,4,256]{2,1,0:T(4,128)S(1)}, f32[4,4,256,64]{2,3,1,0:T(8,128)}, bf16[4,4,256,64]{2,3,1,0:T(8,128)(2,1)S(1)}, bf16[4,64,64]{2,1...) while((s32[]{:T(128)}, f32[4,4,256]{2,1,0:T(4,128)S(1)}, ...), condition=%wide.region_3.4_spmd.clone, body=%wide.region_0.3_spmd.clone.sunk | while | flops 17454080 | bytes 1326441 | solution.py:113
  69.9 0.9 fusion.74
  71.2 0.9 fusion.74
  72.5 0.9 fusion.74
  73.8 0.9 fusion.74
  74.7 0.3 reshape.514
  75.1 1.2 %all-to-all-done.1 = bf16[4,2,16384]{2,1,0:T(2,128)(2,1)S(1)} async-done(((bf16[4,2,16384]{2,1,0:T(2,128)(2,1)}), bf16[4,2,16384]{2,1,0:T(2,128)(2,1)S(1)}, u32[]{:S(2)}, u32[]{:S(2)}) %all-to-all-start.1) | async-done | bytes 262176 | tf_op jit(solution)/shard_map/all_to_all | solution.py:134
  76.3 0.3 reshape.512
  77.0 2.3 %gather_fusion.2 = bf16[128,64,64]{2,1,0:T(8,128)(2,1)} fusion(bf16[4,12,64,64]{3,2,1,0:T(8,128)(2,1)S(1)} %pad_maximum_fusion, s32[128]{0:T(128)S(1)} %reshape.460), kind=kCustom, calls=%fused_computation.2 | custom fusion | bytes 2098176 | tf_op jit(solution)/shard_map/gather | solution.py:145
  79.3 1.1 gather_fusion.4
  80.5 28.3 %while.23 = (s32[]{:T(128)}, f32[2,4,4,128,64]{3,4,2,1,0:T(8,128)}, s32[2,4,16]{2,1,0:T(4,128)S(1)}, s32[2]{0:T(128)S(1)}, s32[]{:T(128)}, /*index=5*/bf16[2,4,1...) while((s32[]{:T(128)}, f32[2,4,4,128,64]{3,4,2,1,0:T(8,128)}, ...), condition=%wide.region_10.11_spmd, body=%wide.region_7.10_spmd.sunk | while | flops 562172224 | bytes 65482908 | solution.py:175
  80.5 0.7 dynamic_slice.83
  82.4 0.9 compare_and_fusion.4
  83.3 1.4 %compare_and_fusion.5 = pred[4,128,1024]{1,2,0:T(8,128)(4,1)S(1)} fusion(s32[128]{0:T(128)S(1)} %iota_add_fusion.5, s32[4,1024]{1,0:T(4,128)S(1)} %broadcast_add_fusion.2, pred[4,1024]{1,0:T(4,128)(4,1)S(1)} %and.110), kind=kLoop, calls=%fused_computation.15.clone.1 | loop fusion | flops 1048576 | bytes 545280 | tf_op jit(solution)/shard_map/while/body/eval_jaxpr/and | solution.py:161
  84.8 2.5 %select_reduce_fusion.5 = (f32[4,4,128]{2,1,0:T(4,128)S(1)}, f32[4,4,128,16,64]{2,4,1,3,0:T(8,128)S(1)}) fusion(pred[4,128,16,64]{1,3,2,0:T(8,128)(4,1)S(1)} %compare_and_fusion.4, bf16[2,128,4,4,64]{1,4,3,2,0:T(8,128)(2,1)} %get-tuple-element.346, s32[]{:T(128)S(6)} %copy.143, bf16[2,4,16,64,64]{4,3,2,1,0:T(8,128)(2,1)} %get-tuple-element.345), kind=kOutput, calls=%fused_computation.13.clone.1 | convolution fusion | flops 274724864 | bytes 10232832 | tf_op jit(solution)/shard_map/while/body/eval_jaxpr/tghd,gnkd->ghtnk/dot_general | solution.py:152
  87.3 2.1 %select_reduce_fusion.6 = f32[4,4,128]{2,1,0:T(4,128)S(1)} fusion(f32[4,4,128,16,64]{2,4,1,3,0:T(8,128)S(1)} %get-tuple-element.306, f32[4,4,128]{2,1,0:T(4,128)S(1)} %get-tuple-element.307, pred[4,128,16,64]{1,3,2,0:T(8,128)(4,1)S(1)} %compare_and_fusion.4), kind=kLoop, calls=%fused_computation.11.clone.1 | loop fusion | flops 8386560 | bytes 8929280 | tf_op jit(solution)/shard_map/while/body/eval_jaxpr/reduce_sum | solution.py:165
  89.4 0.8 copy.137
  90.3 2.4 %fusion.68 = bf16[4,4,128,1024]{2,3,1,0:T(8,128)(2,1)S(1)} fusion(f32[4,4,128,16,64]{2,4,3,1,0:T(8,128)S(1)} %copy.137, f32[4,4,128]{2,1,0:T(4,128)S(1)} %get-tuple-element.307, pred[4,128,1024]{1,2,0:T(8,128)(4,1)S(1)} %compare_and_fusion.5), kind=kLoop, calls=%fused_computation.10.clone.1 | loop fusion | flops 8388608 | bytes 13115392 | tf_op jit(solution)/shard_map/while/body/eval_jaxpr/convert_element_type | solution.py:169
  92.7 0.9 fusion.69
  93.6 1.0 copy-done.1
  94.6 0.7 dynamic_slice.83
  96.5 0.9 compare_and_fusion.4
  97.4 1.4 %compare_and_fusion.5 = pred[4,128,1024]{1,2,0:T(8,128)(4,1)S(1)} fusion(s32[128]{0:T(128)S(1)} %iota_add_fusion.5, s32[4,1024]{1,0:T(4,128)S(1)} %broadcast_add_fusion.2, pred[4,1024]{1,0:T(4,128)(4,1)S(1)} %and.110), kind=kLoop, calls=%fused_computation.15.clone.1 | loop fusion | flops 1048576 | bytes 545280 | tf_op jit(solution)/shard_map/while/body/eval_jaxpr/and | solution.py:161
  98.9 2.5 %select_reduce_fusion.5 = (f32[4,4,128]{2,1,0:T(4,128)S(1)}, f32[4,4,128,16,64]{2,4,1,3,0:T(8,128)S(1)}) fusion(pred[4,128,16,64]{1,3,2,0:T(8,128)(4,1)S(1)} %compare_and_fusion.4, bf16[2,128,4,4,64]{1,4,3,2,0:T(8,128)(2,1)} %get-tuple-element.346, s32[]{:T(128)S(6)} %copy.143, bf16[2,4,16,64,64]{4,3,2,1,0:T(8,128)(2,1)} %get-tuple-element.345), kind=kOutput, calls=%fused_computation.13.clone.1 | convolution fusion | flops 274724864 | bytes 10232832 | tf_op jit(solution)/shard_map/while/body/eval_jaxpr/tghd,gnkd->ghtnk/dot_general | solution.py:152
  101.4 2.1 %select_reduce_fusion.6 = f32[4,4,128]{2,1,0:T(4,128)S(1)} fusion(f32[4,4,128,16,64]{2,4,1,3,0:T(8,128)S(1)} %get-tuple-element.306, f32[4,4,128]{2,1,0:T(4,128)S(1)} %get-tuple-element.307, pred[4,128,16,64]{1,3,2,0:T(8,128)(4,1)S(1)} %compare_and_fusion.4), kind=kLoop, calls=%fused_computation.11.clone.1 | loop fusion | flops 8386560 | bytes 8929280 | tf_op jit(solution)/shard_map/while/body/eval_jaxpr/reduce_sum | solution.py:165
  103.6 0.8 copy.137
  104.4 2.4 %fusion.68 = bf16[4,4,128,1024]{2,3,1,0:T(8,128)(2,1)S(1)} fusion(f32[4,4,128,16,64]{2,4,3,1,0:T(8,128)S(1)} %copy.137, f32[4,4,128]{2,1,0:T(4,128)S(1)} %get-tuple-element.307, pred[4,128,1024]{1,2,0:T(8,128)(4,1)S(1)} %compare_and_fusion.5), kind=kLoop, calls=%fused_computation.10.clone.1 | loop fusion | flops 8388608 | bytes 13115392 | tf_op jit(solution)/shard_map/while/body/eval_jaxpr/convert_element_type | solution.py:169
  106.8 0.9 fusion.69
  107.7 1.0 copy-done.1
  108.7 1.6 %fusion.33 = (f32[256,4,4]{0,2,1:T(4,128)S(1)}, f32[4,4,256,64]{2,3,1,0:T(8,128)S(1)}) fusion(f32[256,4,4]{0,2,1:T(4,128)S(1)} %mul.290, f32[256,4,4]{0,2,1:T(4,128)S(1)} %mul.287, f32[4,4,256,64]{2,3,1,0:T(8,128)S(1)} %copy-done.4, f32[4,4,256]{2,1,0:T(4,128)S(1)} %broadcast_maximum_fusion.1, f32[2,4,4,128,64]{3,4,2,1,0:T(8,128)} %get-tuple-element.87), kind=kLoop, calls=%fused_computation.57 | loop fusion | flops 1568768 | bytes 3211264 | tf_op jit(solution)/shard_map/reduce_sum | solution.py:182
  110.3 2.0 %copy.86 = f32[2,128,4,4,64]{1,0,4,3,2:T(2,128)S(1)} copy(f32[2,128,4,4,64]{1,4,3,2,0:T(8,128)} %bitcast.233) | data formatting | bytes 2097152 | tf_op jit(solution)/shard_map/transpose | solution.py:178
  112.4 0.8 reshape.442
  113.2 0.2 fusion.35
  113.5 1.0 copy.88
  (120 shorter events, 6.2 us)
Async XLA Ops:
  0.0 23.6 %copy-start.5 = (bf16[1,256,1024]{2,1,0:T(8,128)(2,1)S(1)}, bf16[1,256,1024]{2,1,0:T(8,128)(2,1)}, u32[]{:S(2)}) copy-start(bf16[1,256,1024]{2,1,0:T(8,128)(2,1)} %param.12) | copy-start | bytes 1572868
  2.6 23.2 %all-to-all-start = ((s32[4,4,2]{1,2,0:T(2,128)}), s32[4,4,2]{1,2,0:T(2,128)S(1)}, u32[]{:S(2)}, u32[]{:S(2)}) async-start(s32[4,4,2]{1,2,0:T(2,128)} %copy.74), calls=%async_computation | async-start | bytes 8192 | tf_op jit(solution)/shard_map/all_to_all | solution.py:129
  9.6 27.4 %collective-permute-start.1 = (bf16[16,256]{1,0:T(8,128)(2,1)S(1)}, bf16[16,256]{1,0:T(8,128)(2,1)S(1)}, u32[]{:S(2)}, u32[]{:S(2)}) collective-permute-start(bf16[16,256]{1,0:T(8,128)(2,1)S(1)} %slice_bitcast_fusion.1), channel_id=1, source_target_pairs={{2,0},{4,2},{6,4},{3,1},{5,3},{7,5},{10,8},{12,10},{14,12},{11,9},... | collective-permute-start | bytes 24584 | tf_op jit(solution)/shard_map/ppermute | solution.py:21
  11.6 25.8 %collective-permute-start = (bf16[16,256]{1,0:T(8,128)(2,1)S(1)}, bf16[16,256]{1,0:T(8,128)(2,1)S(1)}, u32[]{:S(2)}, u32[]{:S(2)}) collective-permute-start(bf16[16,256]{1,0:T(8,128)(2,1)S(1)} %slice_bitcast_fusion.4), channel_id=1, source_target_pairs={{2,0},{4,2},{6,4},{3,1},{5,3},{7,5},{10,8},{12,10},{14,12},{11,9},... | collective-permute-start | bytes 24584 | tf_op jit(solution)/shard_map/ppermute | solution.py:21
  19.6 17.4 %copy-start.2 = (bf16[1,256,256]{2,1,0:T(8,128)(2,1)S(1)}, bf16[1,256,256]{2,1,0:T(8,128)(2,1)}, u32[]{:S(2)}) copy-start(bf16[1,256,256]{2,1,0:T(8,128)(2,1)} %param.14) | copy-start | bytes 393220
  22.8 14.6 %copy-start.3 = (bf16[1,256,256]{2,1,0:T(8,128)(2,1)S(1)}, bf16[1,256,256]{2,1,0:T(8,128)(2,1)}, u32[]{:S(2)}) copy-start(bf16[1,256,256]{2,1,0:T(8,128)(2,1)} %param.13) | copy-start | bytes 393220
  27.8 37.1 %all-to-all-start.2 = ((bf16[4,2,16384]{2,1,0:T(2,128)(2,1)}), bf16[4,2,16384]{2,1,0:T(2,128)(2,1)S(1)}, u32[]{:S(2)}, u32[]{:S(2)}) async-start(bf16[4,2,16384]{2,1,0:T(2,128)(2,1)} %reshape.513), calls=%async_computation.2 | async-start | bytes 524288 | tf_op jit(solution)/shard_map/all_to_all | solution.py:135
  64.9 11.4 %all-to-all-start.1 = ((bf16[4,2,16384]{2,1,0:T(2,128)(2,1)}), bf16[4,2,16384]{2,1,0:T(2,128)(2,1)S(1)}, u32[]{:S(2)}, u32[]{:S(2)}) async-start(bf16[4,2,16384]{2,1,0:T(2,128)(2,1)} %reshape.511), calls=%async_computation.1 | async-start | bytes 524288 | tf_op jit(solution)/shard_map/all_to_all | solution.py:134
  74.7 5.7 %copy-start.6 = (s32[1,2,4,16]{3,2,1,0:T(4,128)S(1)}, s32[1,2,4,16]{3,2,1,0:T(4,128)}, u32[]{:S(2)}) copy-start(s32[1,2,4,16]{3,2,1,0:T(4,128)} %param.16) | copy-start | bytes 1540
  80.4 28.3 %copy-start.4 = (f32[4,4,256,64]{2,3,1,0:T(8,128)S(1)}, f32[4,4,256,64]{2,3,1,0:T(8,128)}, u32[]{:S(2)}) copy-start(f32[4,4,256,64]{2,3,1,0:T(8,128)} %get-tuple-element.85) | copy-start | bytes 3145732
  80.4 32.8 %copy-start.7 = (f32[1024]{0:T(1024)S(1)}, f32[1024]{0:T(1024)}, u32[]{:S(2)}) copy-start(f32[1024]{0:T(1024)} %param.19) | copy-start | bytes 12292
  90.3 2.4 %copy-start = (f32[2,4,4,128,64]{3,4,2,1,0:T(8,128)S(1)}, f32[2,4,4,128,64]{3,4,2,1,0:T(8,128)}, u32[]{:S(2)}) copy-start(f32[2,4,4,128,64]{3,4,2,1,0:T(8,128)} %get-tuple-element.331) | copy-start | bytes 3145732 | tf_op jit(solution)/shard_map/while
  93.6 1.0 copy-start.1
  104.4 2.4 %copy-start = (f32[2,4,4,128,64]{3,4,2,1,0:T(8,128)S(1)}, f32[2,4,4,128,64]{3,4,2,1,0:T(8,128)}, u32[]{:S(2)}) copy-start(f32[2,4,4,128,64]{3,4,2,1,0:T(8,128)} %get-tuple-element.331) | copy-start | bytes 3145732 | tf_op jit(solution)/shard_map/while
  107.7 1.0 copy-start.1
where the time goes:
time: 115 us; the launch traced here: 114 us
  local copies, waits for them, and re-layouts  29.9 us (26%)
  blocking collectives  27 us (23%)
  other arithmetic  22.1 us (19%)
  starting transfers between devices  21 us (18%)
  matrix products  11.2 us (10%)
  loops' own time  1.71 us (1%)
  waiting for transfers between devices  1.22 us (1%)
    all_gather x1, blocking collectives, per_device(): part_values = lax.all_gather(value_summary, 'kv', axis=0, tiled=True)  13.7 us
    all_gather x1, blocking collectives, per_device(): part_keys = lax.all_gather(key_summary, 'kv', axis=0, tiled=True)  13.3 us
    all_to_all x1, starting transfers between devices, per_device(): lax.all_to_all(served[1], 'kv', split_axis=0, concat_axis=0, tiled=True)  7.44 us
    all_to_all x1, starting transfers between devices, per_device(): lax.all_to_all(asked_ids, 'kv', split_axis=0, concat_axis=0, tiled=True)  6.35 us
    unnamed x21, local copies, waits for them, and re-layouts  5.66 us
    dot_general x2, matrix products, attend(): jnp.einsum('tghd,gnkd->ghtnk', query_part, keys_part, preferred_element_t...  5.03 us
    convert_element_type x2, other arithmetic, attend(): weight.astype(jnp.bfloat16)  4.81 us
    and x4, other arithmetic, attend(): live[:, None, :] & (key_place[:, None, :] <= place_q[None, :, None])  4.65 us
  transfers between devices with their start and end apart: 5, of which 1 were waited for; matrix products, arithmetic and copies ran while one was open for 21% of the time, Pallas kernels for 0%

commit v1 on v0

--- a/solution.py
+++ b/solution.py
@@ -82,7 +82,13 @@
     value_summary = compress(jnp.concatenate([values, next_values], 0), pool_v, groups)
     place = start + jnp.arange(length)
     query_group = queries.reshape(length, groups, per_group, DH).transpose(1, 2, 0, 3)
-    part_keys = lax.all_gather(key_summary, "kv", axis=0, tiled=True)
+    size = lax.axis_size("kv")
+    held, pieces = (key_summary, [key_summary])
+    for _ in range(size - 1):
+        held = lax.ppermute(held, "kv", [(i_2, (i_2 + 1) % size) for i_2 in range(size)])
+        pieces.insert(0, held)
+    row_of_blocks = jnp.concatenate(pieces, axis=0)
+    part_keys = jnp.roll(row_of_blocks, (lax.axis_index("kv") + 1) * key_summary.shape[0], axis=0)
     part_values = lax.all_gather(value_summary, "kv", axis=0, tiled=True)
     count = part_keys.shape[0]
     ends = jnp.arange(count) * CMP_STRIDE + CMP_BLOCK - 1

time: 115 us -> 115 us (level)
  blocking collectives: 27 us -> 13.1 us
  waiting for transfers between devices: 1.22 us -> 9.87 us
  starting transfers between devices: 21 us -> 23.9 us
  local copies, waits for them, and re-layouts: 29.9 us -> 31.6 us
    all_gather x1 -> x0, blocking collectives: 13.3 us -> none  [per_device(): part_keys = lax.all_gather(key_summary, 'kv', axis=0, tiled=True)]
    ppermute x0 -> x3, waiting for transfers between devices: none -> 8.65 us  [per_device(): lax.ppermute(held, 'kv', [(i_2, (i_2 + 1) % size) for i_2 in range(size)])]
    ppermute x0 -> x3, starting transfers between devices: none -> 2.29 us  [per_device(): lax.ppermute(held, 'kv', [(i_2, (i_2 + 1) % size) for i_2 in range(size)])]
    mul x2, local copies, waits for them, and re-layouts: 1.7 us -> 3.3 us  [attend(): score = score.reshape(groups, per_group, QB, NSEL * SLC) * scale]
    unnamed x21 -> x28, local copies, waits for them, and re-layouts: 5.66 us -> 5.74 us
  transfers between devices with their start and end apart: 5 -> 8, of which waited for: 1 -> 3; matrix products, arithmetic and copies ran while one was open for 21% -> 21% of each run, Pallas kernels for 0% -> 0%
where the time goes in v1:
time: 115 us; the launch traced here: 114 us
  local copies, waits for them, and re-layouts  31.6 us (27%)
  starting transfers between devices  23.9 us (21%)
  other arithmetic  22.1 us (19%)
  blocking collectives  13.1 us (11%)
  matrix products  11.1 us (10%)
  waiting for transfers between devices  9.87 us (9%)
  loops' own time  1.71 us (1%)
    all_gather x1, blocking collectives, per_device(): part_values = lax.all_gather(value_summary, 'kv', axis=0, tiled=True)  13.1 us
    ppermute x3, waiting for transfers between devices, per_device(): lax.ppermute(held, 'kv', [(i_2, (i_2 + 1) % size) for i_2 in range(size)])  8.65 us
    all_to_all x1, starting transfers between devices, per_device(): lax.all_to_all(served[1], 'kv', split_axis=0, concat_axis=0, tiled=True)  7.44 us
    all_to_all x1, starting transfers between devices, per_device(): lax.all_to_all(asked_ids, 'kv', split_axis=0, concat_axis=0, tiled=True)  6.35 us
    unnamed x28, local copies, waits for them, and re-layouts  5.74 us
    all_to_all x1, starting transfers between devices, per_device(): lax.all_to_all(served[0], 'kv', split_axis=0, concat_axis=0, tiled=True)  5.29 us
    dot_general x2, matrix products, attend(): jnp.einsum('tghd,gnkd->ghtnk', query_part, keys_part, preferred_element_t...  5.03 us
    convert_element_type x2, other arithmetic, attend(): weight.astype(jnp.bfloat16)  4.81 us
  transfers between devices with their start and end apart: 8, of which 3 were waited for; matrix products, arithmetic and copies ran while one was open for 21% of the time, Pallas kernels for 0%

profile of v1, /device:TPU:0, one launch (start us, length us, event | category | flops | bytes accessed | tf_op | source)
XLA Modules:
  0.0 114.0 jit_solution(4192023715463981987)
XLA Ops:
  0.0 0.8 fusion.37
  0.9 0.7 reduce_window_sum.13
  1.9 0.7 copy.74
  2.6 6.3 %all-to-all-start = ((s32[4,4,2]{1,2,0:T(2,128)}), s32[4,4,2]{1,2,0:T(2,128)S(1)}, u32[]{:S(2)}, u32[]{:S(2)}) async-start(s32[4,4,2]{1,2,0:T(2,128)} %copy.74), calls=%async_computation | async-start | bytes 8192 | tf_op jit(solution)/shard_map/all_to_all | solution.py:135
  8.9 0.7 slice_bitcast_fusion.1
  9.6 1.3 %collective-permute-start.4 = (bf16[16,256]{1,0:T(8,128)(2,1)S(1)}, bf16[16,256]{1,0:T(8,128)(2,1)S(1)}, u32[]{:S(2)}, u32[]{:S(2)}) collective-permute-start(bf16[16,256]{1,0:T(8,128)(2,1)S(1)} %slice_bitcast_fusion.1), channel_id=1, source_target_pairs={{2,0},{4,2},{6,4},{3,1},{5,3},{7,5},{10,8},{12,10},{14,12},{11,9},... | collective-permute-start | bytes 24584 | tf_op jit(solution)/shard_map/ppermute | solution.py:21
  10.9 0.7 slice_bitcast_fusion.4
  11.6 1.3 %collective-permute-start = (bf16[16,256]{1,0:T(8,128)(2,1)S(1)}, bf16[16,256]{1,0:T(8,128)(2,1)S(1)}, u32[]{:S(2)}, u32[]{:S(2)}) collective-permute-start(bf16[16,256]{1,0:T(8,128)(2,1)S(1)} %slice_bitcast_fusion.4), channel_id=1, source_target_pairs={{2,0},{4,2},{6,4},{3,1},{5,3},{7,5},{10,8},{12,10},{14,12},{11,9},... | collective-permute-start | bytes 24584 | tf_op jit(solution)/shard_map/ppermute | solution.py:21
  13.0 0.7 bitcast_or_fusion
  13.8 1.0 copy.73
  14.8 1.1 reshape_squeeze.9
  15.8 1.1 slice.65
  16.9 1.1 slice.72
  18.1 1.5 %gather_fusion.1 = s32[128]{0:T(128)S(1)} fusion(s32[4,16]{1,0:T(4,128)S(1)} %convert_subtract_fusion, s32[128]{0:T(128)S(1)} %reshape.454), kind=kCustom, calls=%fused_computation.1 | custom fusion | bytes 2048 | tf_op jit(solution)/shard_map/gather | solution.py:150
  19.8 0.7 fusion.46
  20.6 0.7 slice_bitcast_fusion.5
  21.3 0.7 slice_bitcast_fusion
  22.0 0.8 add_divide_fusion
  23.4 0.2 copy.77
  24.9 0.9 copy.84
  26.1 0.7 gather_fusion.3
  26.7 1.1 reshape.513
  27.8 7.4 %all-to-all-start.2 = ((bf16[4,2,16384]{2,1,0:T(2,128)(2,1)}), bf16[4,2,16384]{2,1,0:T(2,128)(2,1)S(1)}, u32[]{:S(2)}, u32[]{:S(2)}) async-start(bf16[4,2,16384]{2,1,0:T(2,128)(2,1)} %reshape.513), calls=%async_computation.2 | async-start | bytes 524288 | tf_op jit(solution)/shard_map/all_to_all | solution.py:141
  35.3 0.7 gather_fusion
  36.0 1.1 reshape.511
  37.7 2.1 %collective-permute-start.1 = (bf16[16,4,64]{2,0,1:T(8,128)(2,1)S(1)}, bf16[16,4,64]{2,0,1:T(8,128)(2,1)S(1)}, u32[]{:S(2)}, u32[]{:S(2)}) collective-permute-start(bf16[16,4,64]{2,0,1:T(8,128)(2,1)S(1)} %fusion.40), channel_id=1, source_target_pairs={{0,2},{2,4},{4,6},{6,0},{1,3},{3,5},{5,7},{7,1},{8,10},{10,12},{12... | collective-permute-start | bytes 24584 | tf_op jit(solution)/shard_map/ppermute | solution.py:88
  39.9 3.3 %collective-permute-done.1 = bf16[16,4,64]{2,0,1:T(8,128)(2,1)S(1)} collective-permute-done((bf16[16,4,64]{2,0,1:T(8,128)(2,1)S(1)}, bf16[16,4,64]{2,0,1:T(8,128)(2,1)S(1)}, u32[]{:S(2)}, u32[]{:S(2)}) %collective-permute-start.1) | collective-permute-done | bytes 8224 | tf_op jit(solution)/shard_map/ppermute | solution.py:88
  43.5 5.3 %collective-permute-done.2 = bf16[16,4,64]{2,0,1:T(8,128)(2,1)S(1)} collective-permute-done((bf16[16,4,64]{2,0,1:T(8,128)(2,1)S(1)}, bf16[16,4,64]{2,0,1:T(8,128)(2,1)S(1)}, u32[]{:S(2)}, u32[]{:S(2)}) %collective-permute-start.2) | collective-permute-done | bytes 8224 | tf_op jit(solution)/shard_map/ppermute | solution.py:88
  48.8 13.1 %all_gather.3 = bf16[64,4,64]{2,1,0:T(4,128)(2,1)S(1)} all-gather(bf16[16,4,64]{2,1,0:T(4,128)(2,1)S(1)} %fusion.39), channel_id=1, replica_groups=mesh['grp'=2,'dp'=2,'kv'=4,'tp'=2] {'kv'}, dimensions={0}, use_global_device_ids=true | all-gather | bytes 40960 | tf_op jit(solution)/shard_map/all_gather | solution.py:92
  62.2 5.3 %all-to-all-start.1 = ((bf16[4,2,16384]{2,1,0:T(2,128)(2,1)}), bf16[4,2,16384]{2,1,0:T(2,128)(2,1)S(1)}, u32[]{:S(2)}, u32[]{:S(2)}) async-start(bf16[4,2,16384]{2,1,0:T(2,128)(2,1)} %reshape.511), calls=%async_computation.1 | async-start | bytes 524288 | tf_op jit(solution)/shard_map/all_to_all | solution.py:140
  67.5 5.2 %while.24 = (s32[]{:T(128)}, f32[4,4,256]{2,1,0:T(4,128)S(1)}, f32[4,4,256,64]{2,3,1,0:T(8,128)}, bf16[4,4,256,64]{2,3,1,0:T(8,128)(2,1)S(1)}, bf16[4,64,64]{2,1...) while((s32[]{:T(128)}, f32[4,4,256]{2,1,0:T(4,128)S(1)}, ...), condition=%wide.region_3.4_spmd.clone, body=%wide.region_0.3_spmd.clone.sunk | while | flops 17454080 | bytes 1326441 | solution.py:119
  67.9 0.9 fusion.74
  69.2 0.9 fusion.74
  70.4 0.9 fusion.74
  71.7 0.9 fusion.74
  72.6 0.3 reshape.514
  73.0 1.2 %all-to-all-done.1 = bf16[4,2,16384]{2,1,0:T(2,128)(2,1)S(1)} async-done(((bf16[4,2,16384]{2,1,0:T(2,128)(2,1)}), bf16[4,2,16384]{2,1,0:T(2,128)(2,1)S(1)}, u32[]{:S(2)}, u32[]{:S(2)}) %all-to-all-start.1) | async-done | bytes 262176 | tf_op jit(solution)/shard_map/all_to_all | solution.py:140
  74.2 0.3 reshape.512
  75.0 2.3 %gather_fusion.2 = bf16[128,64,64]{2,1,0:T(8,128)(2,1)} fusion(bf16[4,12,64,64]{3,2,1,0:T(8,128)(2,1)S(1)} %pad_maximum_fusion, s32[128]{0:T(128)S(1)} %reshape.460), kind=kCustom, calls=%fused_computation.2 | custom fusion | bytes 2098176 | tf_op jit(solution)/shard_map/gather | solution.py:151
  77.3 1.1 gather_fusion.4
  78.4 29.8 %while.23 = (s32[]{:T(128)}, f32[2,4,4,128,64]{3,4,2,1,0:T(8,128)}, s32[2,4,16]{2,1,0:T(4,128)S(1)}, s32[2]{0:T(128)S(1)}, s32[]{:T(128)}, /*index=5*/bf16[2,4,1...) while((s32[]{:T(128)}, f32[2,4,4,128,64]{3,4,2,1,0:T(8,128)}, ...), condition=%wide.region_10.11_spmd, body=%wide.region_7.10_spmd.sunk | while | flops 562172224 | bytes 65482908 | solution.py:181
  78.4 0.7 dynamic_slice.89
  80.3 0.9 compare_and_fusion.4
  81.3 1.4 %compare_and_fusion.5 = pred[4,128,1024]{1,2,0:T(8,128)(4,1)S(1)} fusion(s32[128]{0:T(128)S(1)} %iota_add_fusion.5, s32[4,1024]{1,0:T(4,128)S(1)} %broadcast_add_fusion.2, pred[4,1024]{1,0:T(4,128)(4,1)S(1)} %and.117), kind=kLoop, calls=%fused_computation.15.clone.1 | loop fusion | flops 1048576 | bytes 545280 | tf_op jit(solution)/shard_map/while/body/eval_jaxpr/and | solution.py:167
  82.7 2.5 %select_reduce_fusion.5 = (f32[4,4,128]{2,1,0:T(4,128)S(1)}, f32[4,4,128,16,64]{2,4,1,3,0:T(8,128)S(1)}) fusion(pred[4,128,16,64]{1,3,2,0:T(8,128)(4,1)S(1)} %compare_and_fusion.4, bf16[2,128,4,4,64]{1,4,3,2,0:T(8,128)(2,1)} %get-tuple-element.346, s32[]{:T(128)S(6)} %copy.143, bf16[2,4,16,64,64]{4,3,2,1,0:T(8,128)(2,1)} %get-tuple-element.345), kind=kOutput, calls=%fused_computation.13.clone.1 | convolution fusion | flops 274724864 | bytes 10232832 | tf_op jit(solution)/shard_map/while/body/eval_jaxpr/tghd,gnkd->ghtnk/dot_general | solution.py:158
  85.3 2.1 %select_reduce_fusion.6 = f32[4,4,128]{2,1,0:T(4,128)S(1)} fusion(f32[4,4,128,16,64]{2,4,1,3,0:T(8,128)S(1)} %get-tuple-element.306, f32[4,4,128]{2,1,0:T(4,128)S(1)} %get-tuple-element.307, pred[4,128,16,64]{1,3,2,0:T(8,128)(4,1)S(1)} %compare_and_fusion.4), kind=kLoop, calls=%fused_computation.11.clone.1 | loop fusion | flops 8386560 | bytes 8929280 | tf_op jit(solution)/shard_map/while/body/eval_jaxpr/reduce_sum | solution.py:171
  87.4 1.7 %copy.137 = f32[4,4,128,16,64]{2,4,3,1,0:T(8,128)S(1)} copy(f32[4,4,128,16,64]{2,4,1,3,0:T(8,128)S(1)} %get-tuple-element.306) | data formatting | bytes 16777216 | tf_op jit(solution)/shard_map/while/body/eval_jaxpr/mul | solution.py:161
  89.1 2.4 %fusion.68 = bf16[4,4,128,1024]{2,3,1,0:T(8,128)(2,1)S(1)} fusion(f32[4,4,128,16,64]{2,4,3,1,0:T(8,128)S(1)} %copy.137, f32[4,4,128]{2,1,0:T(4,128)S(1)} %get-tuple-element.307, pred[4,128,1024]{1,2,0:T(8,128)(4,1)S(1)} %compare_and_fusion.5), kind=kLoop, calls=%fused_computation.10.clone.1 | loop fusion | flops 8388608 | bytes 13115392 | tf_op jit(solution)/shard_map/while/body/eval_jaxpr/convert_element_type | solution.py:175
  91.5 0.9 fusion.69
  92.3 1.0 copy-done.1
  93.3 0.7 dynamic_slice.89
  95.2 0.9 compare_and_fusion.4
  96.2 1.4 %compare_and_fusion.5 = pred[4,128,1024]{1,2,0:T(8,128)(4,1)S(1)} fusion(s32[128]{0:T(128)S(1)} %iota_add_fusion.5, s32[4,1024]{1,0:T(4,128)S(1)} %broadcast_add_fusion.2, pred[4,1024]{1,0:T(4,128)(4,1)S(1)} %and.117), kind=kLoop, calls=%fused_computation.15.clone.1 | loop fusion | flops 1048576 | bytes 545280 | tf_op jit(solution)/shard_map/while/body/eval_jaxpr/and | solution.py:167
  97.7 2.5 %select_reduce_fusion.5 = (f32[4,4,128]{2,1,0:T(4,128)S(1)}, f32[4,4,128,16,64]{2,4,1,3,0:T(8,128)S(1)}) fusion(pred[4,128,16,64]{1,3,2,0:T(8,128)(4,1)S(1)} %compare_and_fusion.4, bf16[2,128,4,4,64]{1,4,3,2,0:T(8,128)(2,1)} %get-tuple-element.346, s32[]{:T(128)S(6)} %copy.143, bf16[2,4,16,64,64]{4,3,2,1,0:T(8,128)(2,1)} %get-tuple-element.345), kind=kOutput, calls=%fused_computation.13.clone.1 | convolution fusion | flops 274724864 | bytes 10232832 | tf_op jit(solution)/shard_map/while/body/eval_jaxpr/tghd,gnkd->ghtnk/dot_general | solution.py:158
  100.2 2.1 %select_reduce_fusion.6 = f32[4,4,128]{2,1,0:T(4,128)S(1)} fusion(f32[4,4,128,16,64]{2,4,1,3,0:T(8,128)S(1)} %get-tuple-element.306, f32[4,4,128]{2,1,0:T(4,128)S(1)} %get-tuple-element.307, pred[4,128,16,64]{1,3,2,0:T(8,128)(4,1)S(1)} %compare_and_fusion.4), kind=kLoop, calls=%fused_computation.11.clone.1 | loop fusion | flops 8386560 | bytes 8929280 | tf_op jit(solution)/shard_map/while/body/eval_jaxpr/reduce_sum | solution.py:171
  102.3 1.7 %copy.137 = f32[4,4,128,16,64]{2,4,3,1,0:T(8,128)S(1)} copy(f32[4,4,128,16,64]{2,4,1,3,0:T(8,128)S(1)} %get-tuple-element.306) | data formatting | bytes 16777216 | tf_op jit(solution)/shard_map/while/body/eval_jaxpr/mul | solution.py:161
  104.0 2.4 %fusion.68 = bf16[4,4,128,1024]{2,3,1,0:T(8,128)(2,1)S(1)} fusion(f32[4,4,128,16,64]{2,4,3,1,0:T(8,128)S(1)} %copy.137, f32[4,4,128]{2,1,0:T(4,128)S(1)} %get-tuple-element.307, pred[4,128,1024]{1,2,0:T(8,128)(4,1)S(1)} %compare_and_fusion.5), kind=kLoop, calls=%fused_computation.10.clone.1 | loop fusion | flops 8388608 | bytes 13115392 | tf_op jit(solution)/shard_map/while/body/eval_jaxpr/convert_element_type | solution.py:175
  106.4 0.9 fusion.69
  107.3 1.0 copy-done.1
  108.2 1.6 %fusion.33 = (f32[256,4,4]{0,2,1:T(4,128)S(1)}, f32[4,4,256,64]{2,3,1,0:T(8,128)S(1)}) fusion(f32[256,4,4]{0,2,1:T(4,128)S(1)} %mul.294, f32[256,4,4]{0,2,1:T(4,128)S(1)} %mul.291, f32[4,4,256,64]{2,3,1,0:T(8,128)S(1)} %copy-done.4, f32[4,4,256]{2,1,0:T(4,128)S(1)} %broadcast_maximum_fusion.1, f32[2,4,4,128,64]{3,4,2,1,0:T(8,128)} %get-tuple-element.87), kind=kLoop, calls=%fused_computation.57 | loop fusion | flops 1568768 | bytes 3211264 | tf_op jit(solution)/shard_map/reduce_sum | solution.py:188
  109.9 2.0 %copy.86 = f32[2,128,4,4,64]{1,0,4,3,2:T(2,128)S(1)} copy(f32[2,128,4,4,64]{1,4,3,2,0:T(8,128)} %bitcast.234) | data formatting | bytes 2097152 | tf_op jit(solution)/shard_map/transpose | solution.py:184
  111.9 0.8 reshape.442
  112.8 0.2 fusion.35
  113.0 1.0 copy.88
  (134 shorter events, 6.9 us)
Async XLA Ops:
  0.0 23.9 %copy-start.5 = (bf16[1,256,1024]{2,1,0:T(8,128)(2,1)S(1)}, bf16[1,256,1024]{2,1,0:T(8,128)(2,1)}, u32[]{:S(2)}) copy-start(bf16[1,256,1024]{2,1,0:T(8,128)(2,1)} %param.12) | copy-start | bytes 1572868
  2.6 23.2 %all-to-all-start = ((s32[4,4,2]{1,2,0:T(2,128)}), s32[4,4,2]{1,2,0:T(2,128)S(1)}, u32[]{:S(2)}, u32[]{:S(2)}) async-start(s32[4,4,2]{1,2,0:T(2,128)} %copy.74), calls=%async_computation | async-start | bytes 8192 | tf_op jit(solution)/shard_map/all_to_all | solution.py:135
  9.6 27.4 %collective-permute-start.4 = (bf16[16,256]{1,0:T(8,128)(2,1)S(1)}, bf16[16,256]{1,0:T(8,128)(2,1)S(1)}, u32[]{:S(2)}, u32[]{:S(2)}) collective-permute-start(bf16[16,256]{1,0:T(8,128)(2,1)S(1)} %slice_bitcast_fusion.1), channel_id=1, source_target_pairs={{2,0},{4,2},{6,4},{3,1},{5,3},{7,5},{10,8},{12,10},{14,12},{11,9},... | collective-permute-start | bytes 24584 | tf_op jit(solution)/shard_map/ppermute | solution.py:21
  11.6 25.6 %collective-permute-start = (bf16[16,256]{1,0:T(8,128)(2,1)S(1)}, bf16[16,256]{1,0:T(8,128)(2,1)S(1)}, u32[]{:S(2)}, u32[]{:S(2)}) collective-permute-start(bf16[16,256]{1,0:T(8,128)(2,1)S(1)} %slice_bitcast_fusion.4), channel_id=1, source_target_pairs={{2,0},{4,2},{6,4},{3,1},{5,3},{7,5},{10,8},{12,10},{14,12},{11,9},... | collective-permute-start | bytes 24584 | tf_op jit(solution)/shard_map/ppermute | solution.py:21
  19.7 17.4 %copy-start.2 = (bf16[1,256,256]{2,1,0:T(8,128)(2,1)S(1)}, bf16[1,256,256]{2,1,0:T(8,128)(2,1)}, u32[]{:S(2)}) copy-start(bf16[1,256,256]{2,1,0:T(8,128)(2,1)} %param.14) | copy-start | bytes 393220
  22.8 14.5 %copy-start.3 = (bf16[1,256,256]{2,1,0:T(8,128)(2,1)S(1)}, bf16[1,256,256]{2,1,0:T(8,128)(2,1)}, u32[]{:S(2)}) copy-start(bf16[1,256,256]{2,1,0:T(8,128)(2,1)} %param.13) | copy-start | bytes 393220
  27.8 34.3 %all-to-all-start.2 = ((bf16[4,2,16384]{2,1,0:T(2,128)(2,1)}), bf16[4,2,16384]{2,1,0:T(2,128)(2,1)S(1)}, u32[]{:S(2)}, u32[]{:S(2)}) async-start(bf16[4,2,16384]{2,1,0:T(2,128)(2,1)} %reshape.513), calls=%async_computation.2 | async-start | bytes 524288 | tf_op jit(solution)/shard_map/all_to_all | solution.py:141
  37.7 5.6 %collective-permute-start.1 = (bf16[16,4,64]{2,0,1:T(8,128)(2,1)S(1)}, bf16[16,4,64]{2,0,1:T(8,128)(2,1)S(1)}, u32[]{:S(2)}, u32[]{:S(2)}) collective-permute-start(bf16[16,4,64]{2,0,1:T(8,128)(2,1)S(1)} %fusion.40), channel_id=1, source_target_pairs={{0,2},{2,4},{4,6},{6,0},{1,3},{3,5},{5,7},{7,1},{8,10},{10,12},{12... | collective-permute-start | bytes 24584 | tf_op jit(solution)/shard_map/ppermute | solution.py:88
  43.3 5.5 %collective-permute-start.2 = (bf16[16,4,64]{2,0,1:T(8,128)(2,1)S(1)}, bf16[16,4,64]{2,0,1:T(8,128)(2,1)S(1)}, u32[]{:S(2)}, u32[]{:S(2)}) collective-permute-start(bf16[16,4,64]{2,0,1:T(8,128)(2,1)S(1)} %collective-permute-done.1), channel_id=1, source_target_pairs={{0,2},{2,4},{4,6},{6,0},{1,3},{3,5},{5,7},{7,1},{8,10},{10,12},{12... | collective-permute-start | bytes 24584 | tf_op jit(solution)/shard_map/ppermute | solution.py:88
  48.8 13.2 %collective-permute-start.3 = (bf16[16,4,64]{2,0,1:T(8,128)(2,1)S(1)}, bf16[16,4,64]{2,0,1:T(8,128)(2,1)S(1)}, u32[]{:S(2)}, u32[]{:S(2)}) collective-permute-start(bf16[16,4,64]{2,0,1:T(8,128)(2,1)S(1)} %collective-permute-done.2), channel_id=1, source_target_pairs={{0,2},{2,4},{4,6},{6,0},{1,3},{3,5},{5,7},{7,1},{8,10},{10,12},{12... | collective-permute-start | bytes 24584 | tf_op jit(solution)/shard_map/ppermute | solution.py:88
  62.2 12.1 %all-to-all-start.1 = ((bf16[4,2,16384]{2,1,0:T(2,128)(2,1)}), bf16[4,2,16384]{2,1,0:T(2,128)(2,1)S(1)}, u32[]{:S(2)}, u32[]{:S(2)}) async-start(bf16[4,2,16384]{2,1,0:T(2,128)(2,1)} %reshape.511), calls=%async_computation.1 | async-start | bytes 524288 | tf_op jit(solution)/shard_map/all_to_all | solution.py:140
  72.6 5.7 %copy-start.6 = (s32[1,2,4,16]{3,2,1,0:T(4,128)S(1)}, s32[1,2,4,16]{3,2,1,0:T(4,128)}, u32[]{:S(2)}) copy-start(s32[1,2,4,16]{3,2,1,0:T(4,128)} %param.16) | copy-start | bytes 1540
  78.4 29.9 %copy-start.4 = (f32[4,4,256,64]{2,3,1,0:T(8,128)S(1)}, f32[4,4,256,64]{2,3,1,0:T(8,128)}, u32[]{:S(2)}) copy-start(f32[4,4,256,64]{2,3,1,0:T(8,128)} %get-tuple-element.85) | copy-start | bytes 3145732
  78.4 34.4 %copy-start.7 = (f32[1024]{0:T(1024)S(1)}, f32[1024]{0:T(1024)}, u32[]{:S(2)}) copy-start(f32[1024]{0:T(1024)} %param.19) | copy-start | bytes 12292
  89.0 2.4 %copy-start = (f32[2,4,4,128,64]{3,4,2,1,0:T(8,128)S(1)}, f32[2,4,4,128,64]{3,4,2,1,0:T(8,128)}, u32[]{:S(2)}) copy-start(f32[2,4,4,128,64]{3,4,2,1,0:T(8,128)} %get-tuple-element.331) | copy-start | bytes 3145732 | tf_op jit(solution)/shard_map/while
  92.3 1.0 copy-start.1
  104.0 2.4 %copy-start = (f32[2,4,4,128,64]{3,4,2,1,0:T(8,128)S(1)}, f32[2,4,4,128,64]{3,4,2,1,0:T(8,128)}, u32[]{:S(2)}) copy-start(f32[2,4,4,128,64]{3,4,2,1,0:T(8,128)} %get-tuple-element.331) | copy-start | bytes 3145732 | tf_op jit(solution)/shard_map/while
  107.3 1.0 copy-start.1
